TPU v7x, 32 devices: a whole 2x2x4 slice. The times are simulated.
32 devices in a mesh: grp: 2 (over y), fs: 4 (over z), tp: 4 (over x, core).
Axes of the slice: x: 2, y: 2, z: 4, core: 2. Of those that a mesh axis runs over, the one named last changes fastest.
Arguments:
- tokens: bfloat16 [8, 384, 2048], P(('grp', 'fs'), None, 'tp'), parts along dimension 0, may hold values from -16 to 16
- norm_gain: float32 [2048], P('tp'), may hold values from 0.1 to 1.9
- in_weight: bfloat16 [2048, 1024], P('fs', 'tp'), may hold values from -0.125 to 0.125
- pool_weight: bfloat16 [8, 128, 128], P('tp'), may hold values from -0.5 to 0.5
- pool_scale: float32 [1024], P('tp'), may hold values from 0.1 to 1.9
- out_weight: bfloat16 [1024, 2048], P('fs', 'tp'), may hold values from -0.1875 to 0.1875
- ffn_gain: float32 [2048], P('tp'), may hold values from 0.1 to 1.9
- gate_weight: bfloat16 [2048, 5632], P('fs', 'tp'), may hold values from -0.125 to 0.125
- up_weight: bfloat16 [2048, 5632], P('fs', 'tp'), may hold values from -0.125 to 0.125
- down_weight: bfloat16 [5632, 2048], P('tp', 'fs'), may hold values from -0.078125 to 0.078125
Outputs:
- output: bfloat16 [8, 384, 2048], P(('grp', 'fs'), None, 'tp'), parts along dimension 0
There are 2 independent parts, one for each index of `grp`. A program takes and returns all parts, laid end to end along the dimension named above; an argument that names none is the same for every part. Nothing has to cross between parts.
All inputs are finite; a program needn't handle non-finite values.
Results may differ from a plain program's by a relative error of at most 0.009.
Values may be sent and summed in bfloat16 or wider, within the bound.
A program may use at most 64 MiB of HBM per device.

v0:
```python
import jax
import jax.numpy as jnp
from jax import lax
from jax.sharding import PartitionSpec as P

D = 2048
GD = 128
EPSILON = 0.05
HALVES = (1, 2, 4, 8)


def local(
    tokens,
    norm_gain,
    in_weight,
    pool_weight,
    pool_scale,
    out_weight,
    ffn_gain,
    gate_weight,
    up_weight,
    down_weight,
):
    seq_local, length, feat_local = tokens.shape
    stream = tokens.astype(jnp.float32)
    first_square = lax.psum(jnp.sum(stream * stream, axis=-1), "tp")
    normed = (stream * lax.rsqrt(first_square[..., None] / D + EPSILON) * norm_gain).astype(
        jnp.bfloat16
    )
    in_full = lax.all_gather(in_weight, "fs", axis=0, tiled=True)
    channels = in_full.shape[1]
    weight_rows = in_full
    pool_input = jnp.einsum(
        "slk,kc->slc",
        lax.all_gather(normed, "tp", axis=2, tiled=True),
        weight_rows,
        preferred_element_type=jnp.float32,
    ).astype(jnp.bfloat16)
    pool_float = pool_input.astype(jnp.float32)
    group_local = pool_weight.shape[0]
    group_ids = lax.axis_index("tp") * group_local + jnp.arange(channels) // GD
    selector = group_ids % 4
    running = jnp.concatenate(
        [jnp.zeros((seq_local, 1, channels), jnp.float32), jnp.cumsum(pool_float, axis=1)], axis=1
    )
    position = jnp.arange(length)
    window_mean = jnp.zeros_like(pool_float)
    for window_index, half_width in enumerate(HALVES):
        upper_sum = jnp.concatenate(
            [running[:, half_width:], jnp.repeat(running[:, -1:], half_width, axis=1)], axis=1
        )[:, :length]
        lower_sum = jnp.concatenate(
            [
                jnp.zeros((seq_local, half_width, channels), jnp.float32),
                running[:, : length + 1 - half_width],
            ],
            axis=1,
        )[:, :length]
        counts = (
            jnp.minimum(position + half_width, length) - jnp.maximum(position - half_width, 0)
        ).astype(jnp.float32)
        window_mean = jnp.where(
            selector == window_index, (upper_sum - lower_sum) / counts[:, None], window_mean
        )
    deviation = (window_mean - pool_float).astype(jnp.bfloat16)
    grouped = deviation.reshape(seq_local, length, group_local, GD)
    mapped = jnp.einsum("slgc,gcd->slgd", grouped, pool_weight, preferred_element_type=jnp.float32)
    pooled = (mapped.reshape(seq_local, length, channels) * pool_scale).astype(jnp.bfloat16)
    out_full = lax.all_gather(out_weight, "fs", axis=0, tiled=True)
    weight_rows = out_full
    mixed = stream + jnp.einsum(
        "jut,tx->jux",
        lax.all_gather(pooled, "tp", axis=2, tiled=True),
        weight_rows,
        preferred_element_type=jnp.float32,
    )
    second_square = lax.psum(jnp.sum(mixed * mixed, axis=-1), "tp")
    normed_two = (mixed * lax.rsqrt(second_square[..., None] / D + EPSILON) * ffn_gain).astype(
        jnp.bfloat16
    )
    features_full = lax.all_gather(normed_two, "tp", axis=2, tiled=True)
    gate_sum = jnp.einsum(
        "slk,kf->slf",
        features_full,
        lax.all_gather(gate_weight, "fs", axis=0, tiled=True),
        preferred_element_type=jnp.float32,
    )
    up_sum = jnp.einsum(
        "slk,kf->slf",
        features_full,
        lax.all_gather(up_weight, "fs", axis=0, tiled=True),
        preferred_element_type=jnp.float32,
    )
    hidden = (jax.nn.silu(gate_sum) * up_sum).astype(jnp.bfloat16)
    partial_value = jnp.einsum(
        "hor,rn->hon",
        hidden,
        lax.all_gather(down_weight, "fs", axis=1, tiled=True),
        preferred_element_type=jnp.float32,
    )
    summed = lax.psum_scatter(
        partial_value.astype(jnp.bfloat16), "tp", scatter_dimension=2, tiled=True
    ).astype(jnp.float32)
    return (mixed + summed).astype(jnp.bfloat16)


def solution(mesh):
    return jax.shard_map(
        local,
        mesh=mesh,
        in_specs=(
            P(("grp", "fs"), None, "tp"),
            P("tp"),
            P("fs", "tp"),
            P("tp", None, None),
            P("tp"),
            P("fs", "tp"),
            P("tp"),
            P("fs", "tp"),
            P("fs", "tp"),
            P("tp", "fs"),
        ),
        out_specs=P(("grp", "fs"), None, "tp"),
        check_vma=False,
    )
```

profile of v0, /device:TPU:0, one launch (start us, length us, event | category | flops | bytes accessed | tf_op | source)
XLA Modules:
  0.0 485.2 jit_solution(12671679941246397171)
XLA Ops:
  6.5 0.0 copy-start
  6.5 0.0 all-gather.10.cloned.1.call-start
  6.5 0.7 all-gather.10.cloned.1.call-update
  7.3 0.0 all-gather.8.cloned.1.call-start
  7.3 1.2 fusion.17
  8.5 8.4 %psum.14 = f32[1,384]{1,0:T(1,128)S(1)} all-reduce(f32[1,384]{1,0:T(1,128)S(1)} %reduce_sum.23), channel_id=1, replica_groups=mesh['grp'=2,'fs'=4,'tp'=4] {'tp'}, use_global_device_ids=true, to_apply=%region_1.0 | all-reduce | flops 384 | bytes 3072 | tf_op jit(solution)/shard_map/psum | solution.py:26
  16.9 1.9 fusion.19
  18.8 0.0 all-gather.8.cloned.1.call-update
  18.8 0.0 all-gather.12.cloned.1.call-start
  18.8 0.7 all-gather.12.cloned.1.call-update
  19.5 0.0 all-gather.14.cloned.1.call-start
  19.6 20.0 %all-gather.10.cloned.1.call-done = bf16[2048,256]{1,0:T(8,128)(2,1)} async-done(((bf16[512,256]{1,0:T(8,128)(2,1)}), bf16[2048,256]{1,0:T(8,128)(2,1)}) %all-gather.10.cloned.1.call-update) | async-done | bytes 1048592 | tf_op jit(solution)/shard_map/all_gather | solution.py:30
  39.6 20.6 %all-gather.8.cloned.1.call-done = bf16[1,384,2048]{2,1,0:T(8,128)(2,1)} async-done(((bf16[1,384,512]{2,1,0:T(8,128)(2,1)}), bf16[1,384,2048]{2,1,0:T(8,128)(2,1)}) %all-gather.8.cloned.1.call-update) | async-done | bytes 1572880 | tf_op jit(solution)/shard_map/all_gather | solution.py:35
  60.2 2.3 fusion.14
  62.5 0.3 fusion.23
  62.8 0.1 copy.12
  63.0 0.1 fusion.63
  63.1 0.1 fusion.61
  63.1 0.1 fusion.62
  63.2 0.0 copy-start.3
  63.3 0.5 fusion.39
  63.8 0.0 copy-start.1
  63.8 0.1 reshape.225
  63.8 0.0 copy-done
  63.8 0.3 fusion.40
  64.1 0.0 copy-done.3
  64.1 0.1 fusion.38
  64.2 0.0 copy-start.2
  64.2 8.6 %all_gather.26 = bf16[1,384,1024]{1,2,0:T(8,128)(2,1)S(1)} all-gather(bf16[1,384,256]{1,2,0:T(8,128)(2,1)S(1)} %fusion.38), channel_id=1, replica_groups=mesh['grp'=2,'fs'=4,'tp'=4] {'tp'}, dimensions={2}, use_global_device_ids=true | all-gather | bytes 983040 | tf_op jit(solution)/shard_map/all_gather | solution.py:73
  72.8 17.0 %all-gather.12.cloned.1.call-done = bf16[1024,512]{1,0:T(8,128)(2,1)} async-done(((bf16[256,512]{1,0:T(8,128)(2,1)}), bf16[1024,512]{1,0:T(8,128)(2,1)}) %all-gather.12.cloned.1.call-update) | async-done | bytes 1048592 | tf_op jit(solution)/shard_map/all_gather | solution.py:69
  89.8 0.0 copy-done.1
  89.8 1.9 multiply_reduce_fusion
  91.8 6.1 %psum.15 = f32[1,384]{1,0:T(1,128)S(1)} all-reduce(f32[1,384]{1,0:T(1,128)S(1)} %reduce_sum.25), channel_id=1, replica_groups=mesh['grp'=2,'fs'=4,'tp'=4] {'tp'}, use_global_device_ids=true, to_apply=%region_5.6 | all-reduce | flops 384 | bytes 3072 | tf_op jit(solution)/shard_map/psum | solution.py:77
  97.9 0.0 copy-done.2
  97.9 0.9 multiply_convert_fusion
  98.8 0.0 all-gather.14.cloned.1.call-update
  98.8 0.0 all-gather.16.cloned.1.call-start
  98.8 0.5 all-gather.16.cloned.1.call-update
  99.4 0.0 all-gather.18.cloned.1.call-start
  99.4 0.5 all-gather.18.cloned.1.call-update
  99.9 0.0 all-gather.20.cloned.1.call-start
  100.0 0.7 all-gather.20.cloned.1.call-update
  100.7 0.0 reduce-scatter.2.cloned.1.call-start
  100.7 17.0 %all-gather.14.cloned.1.call-done = bf16[1,384,2048]{2,1,0:T(8,128)(2,1)} async-done(((bf16[1,384,512]{2,1,0:T(8,128)(2,1)}), bf16[1,384,2048]{2,1,0:T(8,128)(2,1)}) %all-gather.14.cloned.1.call-update) | async-done | bytes 1572880 | tf_op jit(solution)/shard_map/all_gather | solution.py:81
  117.8 0.0 copy-start.4
  117.8 108.1 %all-gather.16.cloned.1.call-done = bf16[2048,1408]{1,0:T(8,128)(2,1)} async-done(((bf16[512,1408]{1,0:T(8,128)(2,1)}), bf16[2048,1408]{1,0:T(8,128)(2,1)}) %all-gather.16.cloned.1.call-update) | async-done | bytes 5767184 | tf_op jit(solution)/shard_map/all_gather | solution.py:85
  225.9 7.1 %fusion.3 = f32[384,1408]{1,0:T(8,128)} fusion(bf16[2048,1408]{1,0:T(8,128)(2,1)} %all-gather.16.cloned.1.call-done, bf16[1,384,2048]{2,1,0:T(8,128)(2,1)} %all-gather.14.cloned.1.call-done), kind=kOutput, calls=%fused_computation.5 | convolution fusion | flops 2214592512 | bytes 9502720 | tf_op jit(solution)/shard_map/slk,kf->slf/dot_general | solution.py:82
  233.0 99.3 %all-gather.18.cloned.1.call-done = bf16[2048,1408]{1,0:T(8,128)(2,1)} async-done(((bf16[512,1408]{1,0:T(8,128)(2,1)}), bf16[2048,1408]{1,0:T(8,128)(2,1)}) %all-gather.18.cloned.1.call-update) | async-done | bytes 5767184 | tf_op jit(solution)/shard_map/all_gather | solution.py:91
  332.3 106.5 %all-gather.20.cloned.1.call-done = bf16[1408,2048]{1,0:T(8,128)(2,1)} async-done(((bf16[1408,512]{1,0:T(8,128)(2,1)}), bf16[1408,2048]{1,0:T(8,128)(2,1)}) %all-gather.20.cloned.1.call-update) | async-done | bytes 5767184 | tf_op jit(solution)/shard_map/all_gather | solution.py:98
  438.9 0.0 copy-done.4
  438.9 11.3 %fusion.1 = bf16[1,384,2048]{2,1,0:T(8,128)(2,1)} fusion(bf16[1408,2048]{1,0:T(8,128)(2,1)} %all-gather.20.cloned.1.call-done, bf16[2048,1408]{1,0:T(8,128)(2,1)} %all-gather.18.cloned.1.call-done, f32[384,1408]{1,0:T(8,128)} %fusion.3, bf16[1,384,2048]{2,1,0:T(8,128)(2,1)S(1)} %copy-done.4), kind=kOutput, calls=%fused_computation.3 | convolution fusion | flops 4433215488 | bytes 16842752 | tf_op jit(solution)/shard_map/hor,rn->hon/dot_general | solution.py:95
  450.1 0.0 reduce-scatter.2.cloned.1.call-update
  450.2 26.4 %reduce-scatter.2.cloned.1.call-done = bf16[1,384,512]{2,1,0:T(8,128)(2,1)} async-done(((bf16[1,384,2048]{2,1,0:T(8,128)(2,1)}), bf16[1,384,512]{2,1,0:T(8,128)(2,1)}) %reduce-scatter.2.cloned.1.call-update) | async-done | bytes 393232 | tf_op jit(solution)/shard_map/reduce_scatter | solution.py:101
  476.5 1.9 add_convert_fusion
  (17 shorter events, 0.2 us)
Async XLA Ops:
  6.5 57.3 %copy-start = (bf16[2,128,128]{2,1,0:T(8,128)(2,1)S(1)}, bf16[2,128,128]{2,1,0:T(8,128)(2,1)}, u32[]{:S(2)}) copy-start(bf16[2,128,128]{2,1,0:T(8,128)(2,1)} %param.13) | copy-start | bytes 196612
  6.5 33.1 %all-gather.10.cloned.1.call-start = ((), (), s32[]{:S(2)}) async-start(), calls=%async_computation.2 | async-start | bytes 1310720 | tf_op jit(solution)/shard_map/all_gather | solution.py:30
  7.3 53.0 %all-gather.8.cloned.1.call-start = ((), (), s32[]{:S(2)}) async-start(), calls=%async_computation.1 | async-start | bytes 1966080 | tf_op jit(solution)/shard_map/all_gather | solution.py:35
  18.8 71.0 %all-gather.12.cloned.1.call-start = ((), (), s32[]{:S(2)}) async-start(), calls=%async_computation.3 | async-start | bytes 1310720 | tf_op jit(solution)/shard_map/all_gather | solution.py:69
  19.5 98.3 %all-gather.14.cloned.1.call-start = ((), (), s32[]{:S(2)}) async-start(), calls=%async_computation.4 | async-start | bytes 1966080 | tf_op jit(solution)/shard_map/all_gather | solution.py:81
  63.2 0.9 copy-start.3
  63.8 26.1 %copy-start.1 = (bf16[1,384,512]{2,1,0:T(8,128)(2,1)S(1)}, bf16[1,384,512]{2,1,0:T(8,128)(2,1)}, u32[]{:S(2)}) copy-start(bf16[1,384,512]{2,1,0:T(8,128)(2,1)} %param.10) | copy-start | bytes 1179652
  64.2 33.6 %copy-start.2 = (f32[512]{0:T(512)S(1)}, f32[512]{0:T(512)}, u32[]{:S(2)}) copy-start(f32[512]{0:T(512)} %param.16) | copy-start | bytes 6148
  98.8 127.2 %all-gather.16.cloned.1.call-start = ((), (), s32[]{:S(2)}) async-start(), calls=%async_computation.5 | async-start | bytes 7208960 | tf_op jit(solution)/shard_map/all_gather | solution.py:85
  99.4 233.0 %all-gather.18.cloned.1.call-start = ((), (), s32[]{:S(2)}) async-start(), calls=%async_computation.6 | async-start | bytes 7208960 | tf_op jit(solution)/shard_map/all_gather | solution.py:91
  99.9 338.9 %all-gather.20.cloned.1.call-start = ((), (), s32[]{:S(2)}) async-start(), calls=%async_computation.7 | async-start | bytes 7208960 | tf_op jit(solution)/shard_map/all_gather | solution.py:98
  100.7 375.8 %reduce-scatter.2.cloned.1.call-start = ((), (), s32[]{:S(2)}) async-start(), calls=%async_computation.8 | async-start | bytes 1966080 | tf_op jit(solution)/shard_map/reduce_scatter | solution.py:101
  117.8 321.1 %copy-start.4 = (bf16[1,384,2048]{2,1,0:T(8,128)(2,1)S(1)}, bf16[1,384,2048]{2,1,0:T(8,128)(2,1)}, u32[]{:S(2)}) copy-start(bf16[1,384,2048]{2,1,0:T(8,128)(2,1)} %all-gather.14.cloned.1.call-done) | copy-start | bytes 4718596
Sparse Core Ops, SparseCore 0:
  8.9 30.6 all-gather.9
  41.2 18.9 all-gather.7
  61.8 27.9 all-gather.11
  98.9 18.8 all-gather.13
  119.2 106.6 all-gather.15
  227.4 104.9 all-gather.17
  333.9 104.9 all-gather.19
  450.3 26.2 reduce-scatter.1
where the time goes:
time: 486 us; the launch traced here: 485 us
  waiting for transfers between devices  418 us (86%)
  blocking collectives  23 us (5%)
  matrix products  22.8 us (5%)
  between operations  13.7 us (3%)
  other arithmetic  6.86 us (1%)
    all_gather x1, waiting for transfers between devices, local(): lax.all_gather(gate_weight, 'fs', axis=0, tiled=True)  108 us
    all_gather x1, waiting for transfers between devices, local(): lax.all_gather(down_weight, 'fs', axis=1, tiled=True)  107 us
    all_gather x1, waiting for transfers between devices, local(): lax.all_gather(up_weight, 'fs', axis=0, tiled=True)  99.3 us
    reduce_scatter x1, waiting for transfers between devices, local(): lax.psum_scatter(partial_value.astype(jnp.bfloat16), 'tp', scatter_dimens...  26.4 us
    all_gather x1, waiting for transfers between devices, local(): lax.all_gather(normed, 'tp', axis=2, tiled=True)  20.6 us
    all_gather x1, waiting for transfers between devices, local(): in_full = lax.all_gather(in_weight, 'fs', axis=0, tiled=True)  20 us
    all_gather x1, waiting for transfers between devices, local(): features_full = lax.all_gather(normed_two, 'tp', axis=2, tiled=True)  17 us
    all_gather x1, waiting for transfers between devices, local(): out_full = lax.all_gather(out_weight, 'fs', axis=0, tiled=True)  17 us
  transfers between devices with their start and end apart: 8, of which 8 were waited for; matrix products, arithmetic and copies ran while one was open for 3% of the time, Pallas kernels for 0%

commit v1 on v0

--- a/solution.py
+++ b/solution.py
@@ -85,12 +85,37 @@
         lax.all_gather(gate_weight, "fs", axis=0, tiled=True),
         preferred_element_type=jnp.float32,
     )
+    size, place, width = (lax.axis_size("fs"), lax.axis_index("fs"), up_weight.shape[0])
+    forward = [(i, (i + 1) % size) for i in range(size)]
+    backward = [(i, (i - 1) % size) for i in range(size)]
+    half = size // 2
+    from_left = from_right = up_weight
     up_sum = jnp.einsum(
         "slk,kf->slf",
-        features_full,
-        lax.all_gather(up_weight, "fs", axis=0, tiled=True),
+        lax.dynamic_slice_in_dim(features_full, place * width, up_weight.shape[0], axis=2),
+        up_weight,
         preferred_element_type=jnp.float32,
     )
+    for step in range(1, half + 1):
+        from_left = lax.ppermute(from_left, "fs", forward)
+        if step < size - half:
+            from_right = lax.ppermute(from_right, "fs", backward)
+            up_sum = up_sum + jnp.einsum(
+                "slk,kf->slf",
+                lax.dynamic_slice_in_dim(
+                    features_full, (place + step) % size * width, from_right.shape[0], axis=2
+                ),
+                from_right,
+                preferred_element_type=jnp.float32,
+            )
+        up_sum = up_sum + jnp.einsum(
+            "slk,kf->slf",
+            lax.dynamic_slice_in_dim(
+                features_full, (place - step) % size * width, from_left.shape[0], axis=2
+            ),
+            from_left,
+            preferred_element_type=jnp.float32,
+        )
     hidden = (jax.nn.silu(gate_sum) * up_sum).astype(jnp.bfloat16)
     partial_value = jnp.einsum(
         "hor,rn->hon",

time: 486 us -> 440 us (0.905)
  waiting for transfers between devices: 418 us -> 352 us
  starting transfers between devices: 0.28 us -> 17.4 us
    ppermute x0 -> x3, waiting for transfers between devices: none -> 134 us  [the longest x1 97.8 us: local(): from_right = lax.ppermute(from_right, 'fs', backward)]
    all_gather x1 -> x0, waiting for transfers between devices: 99.3 us -> none  [local(): lax.all_gather(up_weight, 'fs', axis=0, tiled=True)]
    all_gather x1, waiting for transfers between devices: 108 us -> 31.8 us  [local(): lax.all_gather(gate_weight, 'fs', axis=0, tiled=True)]
    ppermute x0 -> x3, starting transfers between devices: none -> 17.1 us  [the longest x2 14.5 us: local(): from_left = lax.ppermute(from_left, 'fs', forward)]
    all_gather x1, waiting for transfers between devices: 17 us -> 0.01 us  [local(): features_full = lax.all_gather(normed_two, 'tp', axis=2, tiled=True)]
    all_gather x1, waiting for transfers between devices: 107 us -> 99.7 us  [local(): lax.all_gather(down_weight, 'fs', axis=1, tiled=True)]
    dot_general x0 -> x3, matrix products: none -> 6.22 us  [the longest x2 4.33 us: local(): jnp.einsum('slk,kf->slf', lax.dynamic_slice_in_dim(features_full, (place...]
  transfers between devices with their start and end apart: 8 -> 10, of which waited for: 8 -> 8; matrix products, arithmetic and copies ran while one was open for 3% -> 5% of each run, Pallas kernels for 0% -> 0%
where the time goes in v1:
time: 440 us
  waiting for transfers between devices  352 us (80%)
  matrix products  26.2 us (6%)
  blocking collectives  23 us (5%)
  starting transfers between devices  17.4 us (4%)
  between operations  13.7 us (3%)
  other arithmetic  6.85 us (2%)
    all_gather x1, waiting for transfers between devices, local(): lax.all_gather(down_weight, 'fs', axis=1, tiled=True)  99.7 us
    ppermute x1, waiting for transfers between devices, local(): from_right = lax.ppermute(from_right, 'fs', backward)  97.8 us
    ppermute x2, waiting for transfers between devices, local(): from_left = lax.ppermute(from_left, 'fs', forward)  36.4 us
    all_gather x1, waiting for transfers between devices, local(): lax.all_gather(gate_weight, 'fs', axis=0, tiled=True)  31.8 us
    reduce_scatter x1, waiting for transfers between devices, local(): lax.psum_scatter(partial_value.astype(jnp.bfloat16), 'tp', scatter_dimens...  26.4 us
    all_gather x1, waiting for transfers between devices, local(): lax.all_gather(normed, 'tp', axis=2, tiled=True)  20.6 us
    all_gather x1, waiting for transfers between devices, local(): in_full = lax.all_gather(in_weight, 'fs', axis=0, tiled=True)  20 us
    all_gather x1, waiting for transfers between devices, local(): out_full = lax.all_gather(out_weight, 'fs', axis=0, tiled=True)  17 us
  transfers between devices with their start and end apart: 10, of which 8 were waited for; matrix products, arithmetic and copies ran while one was open for 5% of the time, Pallas kernels for 0%

profile of v1, /device:TPU:0, one launch (start us, length us, event | category | flops | bytes accessed | tf_op | source)
XLA Modules:
  0.0 439.8 jit_solution(17073644510114031916)
XLA Ops:
  6.5 0.0 copy-start
  6.5 0.0 all-gather.9.cloned.1.call-start
  6.5 0.7 all-gather.9.cloned.1.call-update
  7.3 0.0 all-gather.7.cloned.1.call-start
  7.3 1.2 fusion.18
  8.5 8.4 %psum.14 = f32[1,384]{1,0:T(1,128)S(1)} all-reduce(f32[1,384]{1,0:T(1,128)S(1)} %reduce_sum.23), channel_id=1, replica_groups=mesh['grp'=2,'fs'=4,'tp'=4] {'tp'}, use_global_device_ids=true, to_apply=%region_1.0 | all-reduce | flops 384 | bytes 3072 | tf_op jit(solution)/shard_map/psum | solution.py:26
  16.9 1.9 fusion.20
  18.8 0.0 all-gather.7.cloned.1.call-update
  18.8 0.0 all-gather.11.cloned.1.call-start
  18.8 0.7 all-gather.11.cloned.1.call-update
  19.5 0.0 all-gather.13.cloned.1.call-start
  19.6 20.0 %all-gather.9.cloned.1.call-done = bf16[2048,256]{1,0:T(8,128)(2,1)} async-done(((bf16[512,256]{1,0:T(8,128)(2,1)}), bf16[2048,256]{1,0:T(8,128)(2,1)}) %all-gather.9.cloned.1.call-update) | async-done | bytes 1048592 | tf_op jit(solution)/shard_map/all_gather | solution.py:30
  39.6 20.6 %all-gather.7.cloned.1.call-done = bf16[1,384,2048]{2,1,0:T(8,128)(2,1)} async-done(((bf16[1,384,512]{2,1,0:T(8,128)(2,1)}), bf16[1,384,2048]{2,1,0:T(8,128)(2,1)}) %all-gather.7.cloned.1.call-update) | async-done | bytes 1572880 | tf_op jit(solution)/shard_map/all_gather | solution.py:35
  60.2 2.3 fusion.14
  62.5 0.3 fusion.22
  62.8 0.1 copy.12
  63.0 0.1 fusion.78
  63.1 0.1 fusion.76
  63.1 0.1 fusion.77
  63.2 0.0 copy-start.5
  63.3 0.5 fusion.49
  63.8 0.0 copy-start.1
  63.8 0.1 reshape.242
  63.8 0.0 copy-done
  63.8 0.3 fusion.50
  64.1 0.0 copy-done.5
  64.1 0.1 fusion.37
  64.2 8.6 %all_gather.23 = bf16[1,384,1024]{1,2,0:T(8,128)(2,1)S(1)} all-gather(bf16[1,384,256]{1,2,0:T(8,128)(2,1)S(1)} %fusion.37), channel_id=1, replica_groups=mesh['grp'=2,'fs'=4,'tp'=4] {'tp'}, dimensions={2}, use_global_device_ids=true | all-gather | bytes 983040 | tf_op jit(solution)/shard_map/all_gather | solution.py:73
  72.8 0.0 copy-start.4
  72.8 17.0 %all-gather.11.cloned.1.call-done = bf16[1024,512]{1,0:T(8,128)(2,1)} async-done(((bf16[256,512]{1,0:T(8,128)(2,1)}), bf16[1024,512]{1,0:T(8,128)(2,1)}) %all-gather.11.cloned.1.call-update) | async-done | bytes 1048592 | tf_op jit(solution)/shard_map/all_gather | solution.py:69
  89.8 0.0 copy-done.1
  89.8 1.9 multiply_reduce_fusion
  91.8 6.1 %psum.15 = f32[1,384]{1,0:T(1,128)S(1)} all-reduce(f32[1,384]{1,0:T(1,128)S(1)} %reduce_sum.25), channel_id=1, replica_groups=mesh['grp'=2,'fs'=4,'tp'=4] {'tp'}, use_global_device_ids=true, to_apply=%region_5.6 | all-reduce | flops 384 | bytes 3072 | tf_op jit(solution)/shard_map/psum | solution.py:77
  97.9 0.0 copy-done.4
  97.9 0.9 multiply_convert_fusion
  98.8 0.0 copy-start.2
  98.8 0.0 all-gather.13.cloned.1.call-update
  98.8 0.0 all-gather.15.cloned.1.call-start
  98.8 0.5 all-gather.15.cloned.1.call-update
  99.4 0.0 all-gather.17.cloned.1.call-start
  99.4 0.5 all-gather.17.cloned.1.call-update
  100.0 0.0 reduce-scatter.2.cloned.1.call-start
  100.0 0.1 copy-done.2
  100.1 1.1 collective-permute-start.1
  101.3 2.7 collective-permute-start
  103.9 36.4 %collective-permute-done.1 = bf16[512,1408]{1,0:T(8,128)(2,1)} collective-permute-done((bf16[512,1408]{1,0:T(8,128)(2,1)S(1)}, bf16[512,1408]{1,0:T(8,128)(2,1)}, u32[]{:S(2)}, u32[]{:S(2)}) %collective-permute-start.1) | collective-permute-done | bytes 1441824 | tf_op jit(solution)/shard_map/ppermute | solution.py:100
  140.3 13.3 %collective-permute-start.2 = (bf16[512,1408]{1,0:T(8,128)(2,1)}, bf16[512,1408]{1,0:T(8,128)(2,1)}, u32[]{:S(2)}, u32[]{:S(2)}) collective-permute-start(bf16[512,1408]{1,0:T(8,128)(2,1)} %collective-permute-done.1), channel_id=1, source_target_pairs={{0,4},{4,8},{8,12},{12,0},{1,5},{5,9},{9,13},{13,1},{2,6},{6,10},{... | collective-permute-start | bytes 4325384 | tf_op jit(solution)/shard_map/ppermute | solution.py:100
  153.7 0.0 all-gather.13.cloned.1.call-done
  153.7 0.0 copy-start.3
  153.7 1.9 fusion.42
  155.5 97.8 %collective-permute-done = bf16[512,1408]{1,0:T(8,128)(2,1)} collective-permute-done((bf16[512,1408]{1,0:T(8,128)(2,1)S(1)}, bf16[512,1408]{1,0:T(8,128)(2,1)}, u32[]{:S(2)}, u32[]{:S(2)}) %collective-permute-start) | collective-permute-done | bytes 1441824 | tf_op jit(solution)/shard_map/ppermute | solution.py:102
  253.4 0.0 copy-done.3
  253.4 2.2 convolution_add_fusion.2
  255.5 2.2 convolution_add_fusion.1
  257.7 31.8 %all-gather.15.cloned.1.call-done = bf16[2048,1408]{1,0:T(8,128)(2,1)} async-done(((bf16[512,1408]{1,0:T(8,128)(2,1)}), bf16[2048,1408]{1,0:T(8,128)(2,1)}) %all-gather.15.cloned.1.call-update) | async-done | bytes 5767184 | tf_op jit(solution)/shard_map/all_gather | solution.py:85
  289.5 7.2 %fusion.3 = f32[384,1408]{1,0:T(8,128)} fusion(bf16[2048,1408]{1,0:T(8,128)(2,1)} %all-gather.15.cloned.1.call-done, bf16[1,384,2048]{2,1,0:T(8,128)(2,1)} %all-gather.13.cloned.1.call-done), kind=kOutput, calls=%fused_computation.7 | convolution fusion | flops 2214592512 | bytes 9502720 | tf_op jit(solution)/shard_map/slk,kf->slf/dot_general | solution.py:82
  296.7 0.0 collective-permute-done.2
  296.7 99.7 %all-gather.17.cloned.1.call-done = bf16[1408,2048]{1,0:T(8,128)(2,1)} async-done(((bf16[1408,512]{1,0:T(8,128)(2,1)}), bf16[1408,2048]{1,0:T(8,128)(2,1)}) %all-gather.17.cloned.1.call-update) | async-done | bytes 5767184 | tf_op jit(solution)/shard_map/all_gather | solution.py:123
  396.4 8.3 %fusion.2 = bf16[1,384,2048]{2,1,0:T(8,128)(2,1)} fusion(bf16[1408,2048]{1,0:T(8,128)(2,1)} %all-gather.17.cloned.1.call-done, f32[384,1408]{1,0:T(8,128)S(1)} %convolution_add_fusion.1, bf16[512,1408]{1,0:T(8,128)(2,1)} %collective-permute-done.2, f32[384,1408]{1,0:T(8,128)} %fusion.3, bf16[1,384,2048]{2,1,0:T(8,128)(2,1)} %all-gather.13.cloned.1.call-done, ...), kind=kOutput, calls=%fused_computation.6 | convolution fusion | flops 2772811776 | bytes 13500420 | tf_op jit(solution)/shard_map/hor,rn->hon/dot_general | solution.py:120
  404.7 0.0 reduce-scatter.2.cloned.1.call-update
  404.7 26.4 %reduce-scatter.2.cloned.1.call-done = bf16[1,384,512]{2,1,0:T(8,128)(2,1)} async-done(((bf16[1,384,2048]{2,1,0:T(8,128)(2,1)}), bf16[1,384,512]{2,1,0:T(8,128)(2,1)}) %reduce-scatter.2.cloned.1.call-update) | async-done | bytes 393232 | tf_op jit(solution)/shard_map/reduce_scatter | solution.py:126
  431.1 1.9 add_convert_fusion
  (17 shorter events, 0.2 us)
Async XLA Ops:
  6.5 57.3 %copy-start = (bf16[2,128,128]{2,1,0:T(8,128)(2,1)S(1)}, bf16[2,128,128]{2,1,0:T(8,128)(2,1)}, u32[]{:S(2)}) copy-start(bf16[2,128,128]{2,1,0:T(8,128)(2,1)} %param.13) | copy-start | bytes 196612
  6.5 33.1 %all-gather.9.cloned.1.call-start = ((), (), s32[]{:S(2)}) async-start(), calls=%async_computation.2 | async-start | bytes 1310720 | tf_op jit(solution)/shard_map/all_gather | solution.py:30
  7.3 53.0 %all-gather.7.cloned.1.call-start = ((), (), s32[]{:S(2)}) async-start(), calls=%async_computation.1 | async-start | bytes 1966080 | tf_op jit(solution)/shard_map/all_gather | solution.py:35
  18.8 71.0 %all-gather.11.cloned.1.call-start = ((), (), s32[]{:S(2)}) async-start(), calls=%async_computation.3 | async-start | bytes 1310720 | tf_op jit(solution)/shard_map/all_gather | solution.py:69
  19.5 134.1 %all-gather.13.cloned.1.call-start = ((), (), s32[]{:S(2)}) async-start(), calls=%async_computation.4 | async-start | bytes 1966080 | tf_op jit(solution)/shard_map/all_gather | solution.py:81
  63.2 0.9 copy-start.5
  63.8 26.1 %copy-start.1 = (bf16[1,384,512]{2,1,0:T(8,128)(2,1)S(1)}, bf16[1,384,512]{2,1,0:T(8,128)(2,1)}, u32[]{:S(2)}) copy-start(bf16[1,384,512]{2,1,0:T(8,128)(2,1)} %param.10) | copy-start | bytes 1179652
  72.8 25.1 %copy-start.4 = (f32[512]{0:T(512)S(1)}, f32[512]{0:T(512)}, u32[]{:S(2)}) copy-start(f32[512]{0:T(512)} %param.16) | copy-start | bytes 6148
  98.8 1.4 copy-start.2
  98.8 190.7 %all-gather.15.cloned.1.call-start = ((), (), s32[]{:S(2)}) async-start(), calls=%async_computation.5 | async-start | bytes 7208960 | tf_op jit(solution)/shard_map/all_gather | solution.py:85
  99.4 297.0 %all-gather.17.cloned.1.call-start = ((), (), s32[]{:S(2)}) async-start(), calls=%async_computation.6 | async-start | bytes 7208960 | tf_op jit(solution)/shard_map/all_gather | solution.py:123
  100.0 331.2 %reduce-scatter.2.cloned.1.call-start = ((), (), s32[]{:S(2)}) async-start(), calls=%async_computation.7 | async-start | bytes 1966080 | tf_op jit(solution)/shard_map/reduce_scatter | solution.py:126
  100.1 40.2 %collective-permute-start.1 = (bf16[512,1408]{1,0:T(8,128)(2,1)S(1)}, bf16[512,1408]{1,0:T(8,128)(2,1)}, u32[]{:S(2)}, u32[]{:S(2)}) collective-permute-start(bf16[512,1408]{1,0:T(8,128)(2,1)S(1)} %copy-done.2), channel_id=1, source_target_pairs={{0,4},{4,8},{8,12},{12,0},{1,5},{5,9},{9,13},{13,1},{2,6},{6,10},{... | collective-permute-start | bytes 4325384 | tf_op jit(solution)/shard_map/ppermute | solution.py:100
  101.3 152.1 %collective-permute-start = (bf16[512,1408]{1,0:T(8,128)(2,1)S(1)}, bf16[512,1408]{1,0:T(8,128)(2,1)}, u32[]{:S(2)}, u32[]{:S(2)}) collective-permute-start(bf16[512,1408]{1,0:T(8,128)(2,1)S(1)} %copy-done.2), channel_id=1, source_target_pairs={{0,12},{4,0},{8,4},{12,8},{1,13},{5,1},{9,5},{13,9},{2,14},{6,2},{... | collective-permute-start | bytes 4325384 | tf_op jit(solution)/shard_map/ppermute | solution.py:102
  140.3 156.4 %collective-permute-start.2 = (bf16[512,1408]{1,0:T(8,128)(2,1)}, bf16[512,1408]{1,0:T(8,128)(2,1)}, u32[]{:S(2)}, u32[]{:S(2)}) collective-permute-start(bf16[512,1408]{1,0:T(8,128)(2,1)} %collective-permute-done.1), channel_id=1, source_target_pairs={{0,4},{4,8},{8,12},{12,0},{1,5},{5,9},{9,13},{13,1},{2,6},{6,10},{... | collective-permute-start | bytes 4325384 | tf_op jit(solution)/shard_map/ppermute | solution.py:100
  153.7 99.7 %copy-start.3 = (bf16[1,384,2048]{2,1,0:T(8,128)(2,1)S(1)}, bf16[1,384,2048]{2,1,0:T(8,128)(2,1)}, u32[]{:S(2)}) copy-start(bf16[1,384,2048]{2,1,0:T(8,128)(2,1)} %all-gather.13.cloned.1.call-done) | copy-start | bytes 4718596
Sparse Core Ops, SparseCore 0:
  8.9 30.6 all-gather.8
  41.2 18.9 all-gather.6
  61.8 27.9 all-gather.10
  98.9 18.8 all-gather.12
  119.2 170.2 all-gather.14
  290.9 105.3 all-gather.16
  404.8 26.2 reduce-scatter.1
